TPU v7x, 32 devices: a whole 2x2x4 slice. The times are simulated.
32 devices in a mesh: sp: 8 (over z, y), tp: 4 (over x, core).
Axes of the slice: x: 2, y: 2, z: 4, core: 2. Of those that a mesh axis runs over, the one named last changes fastest.
Arguments:
- layer_input: bfloat16 [8, 1024, 2048], P(None, ('sp', 'tp')), may hold values from -6 to 6
- input_gain: float32 [2048], replicated, may hold values from 0.5 to 1.5
- narrowing_matrix: bfloat16 [2048, 512], replicated, may hold values from -0.125 to 0.125
- rotary_down: bfloat16 [2048, 64], replicated, may hold values from -0.125 to 0.125
- summary_scaling: float32 [512], replicated, may hold values from 0.5 to 1.5
- lookup_widening: bfloat16 [512, 16, 128], P('tp'), may hold values from -0.25 to 0.25
- payload_widening: bfloat16 [512, 16, 128], P('tp'), may hold values from -0.25 to 0.25
- query_nope: bfloat16 [8, 16, 128], P('sp', 'tp'), may hold values from -6 to 6
- query_rotary: bfloat16 [8, 16, 64], P('sp', 'tp'), may hold values from -6 to 6
Outputs:
- stored_summaries: bfloat16 [8, 1024, 512], P('sp', None, 'tp')
- rotary_cache: bfloat16 [8, 1024, 64], P('sp', None, 'tp')
- first_read: bfloat16 [8, 16, 128], P('sp', 'tp')
All inputs are finite; a program needn't handle non-finite values.
Results may differ from a plain program's by a relative error of at most 0.02.
Values may be sent and summed in bfloat16 or wider, within the bound.
A program may use at most 64 MiB of HBM per device.

v0:
```python
import jax
import jax.numpy as jnp
from jax import lax
from jax.sharding import PartitionSpec as P

QK_ROPE = 64
PLAIN_MATCH_SPAN = 128
norm_eps = 1e-06
rotary_base = 10000.0


def summed_rows(portion, width, axis):
    count = width * lax.axis_size(axis)
    return lax.psum_scatter(portion(jnp.int32(0), count), axis, scatter_dimension=0, tiled=True)


def rescaled_lines(vector):
    return vector * lax.rsqrt(jnp.mean(vector * vector, axis=-1, keepdims=True) + norm_eps)


def rotate(vector, position):
    half_width = vector.shape[-1] // 2
    frequency = 1.0 / rotary_base ** (
        jnp.arange(half_width, dtype=jnp.float32) * 2.0 / vector.shape[-1]
    )
    angles = position * frequency
    first_half = vector[..., :half_width]
    second_half = vector[..., half_width:]
    return jnp.concatenate(
        [
            first_half * jnp.cos(angles) - second_half * jnp.sin(angles),
            second_half * jnp.cos(angles) + first_half * jnp.sin(angles),
        ],
        axis=-1,
    )


def to_pieces(array, sp_count, tp_count):
    seq_count, pos_local, cache_width = array.shape
    seq_each = seq_count // sp_count
    width_each = cache_width // tp_count
    array = array.reshape(sp_count, seq_each, pos_local, tp_count, width_each)
    array = array.transpose(0, 3, 1, 2, 4)
    return array.reshape(sp_count * tp_count, seq_each, pos_local, width_each)


def shards(
    layer_input,
    input_gain,
    narrowing_matrix,
    rotary_down,
    summary_scaling,
    lookup_widening,
    payload_widening,
    query_nope,
    query_rotary,
):
    seq_count, pos_local, feature_width = layer_input.shape
    sp_count = lax.axis_size("sp")
    tp_count = lax.axis_size("tp")
    block_index = lax.axis_index(("sp", "tp"))
    normed = (rescaled_lines(layer_input.astype(jnp.float32)) * input_gain).astype(jnp.bfloat16)
    flat_rows = normed.reshape(seq_count * pos_local, feature_width)
    hidden_summary = jnp.dot(
        flat_rows, narrowing_matrix, preferred_element_type=jnp.float32
    ).astype(jnp.bfloat16)
    rotary = jnp.dot(flat_rows, rotary_down, preferred_element_type=jnp.float32).astype(
        jnp.bfloat16
    )
    hidden_summary = (
        (rescaled_lines(hidden_summary.astype(jnp.float32)) * summary_scaling)
        .astype(jnp.bfloat16)
        .reshape(seq_count, pos_local, -1)
    )
    positions = (block_index * pos_local + jnp.arange(pos_local, dtype=jnp.int32)).astype(
        jnp.float32
    )[None, :, None]
    rotary = rotate(rotary.astype(jnp.float32).reshape(seq_count, pos_local, -1), positions).astype(
        jnp.bfloat16
    )
    moved = (
        lax.all_to_all(
            to_pieces(hidden_summary, sp_count, tp_count),
            ("sp", "tp"),
            split_axis=0,
            concat_axis=2,
            tiled=True,
        ),
        lax.all_to_all(
            to_pieces(rotary, sp_count, tp_count),
            ("sp", "tp"),
            split_axis=0,
            concat_axis=2,
            tiled=True,
        ),
    )
    hidden_summary = moved[0][0]
    rotary = moved[1][0]
    pos_total = hidden_summary.shape[1]
    rot_each = rotary.shape[2]
    head_each = query_nope.shape[1]
    query_all, turn_all = (
        lax.all_gather(query_nope, "tp", axis=1, tiled=True),
        lax.all_gather(query_rotary, "tp", axis=1, tiled=True),
    )
    absorbed = jnp.einsum(
        "shd,chd->shc", query_all, lookup_widening, preferred_element_type=jnp.float32
    ).astype(jnp.bfloat16)
    query_turned = rotate(turn_all.astype(jnp.float32), jnp.float32(pos_total)).astype(jnp.bfloat16)
    turned_mine = lax.dynamic_slice_in_dim(
        query_turned, lax.axis_index("tp") * rot_each, rot_each, 2
    )
    score_scale = (PLAIN_MATCH_SPAN + QK_ROPE) ** (-0.5)
    partial_value = (
        jnp.einsum("shc,spc->shp", absorbed, hidden_summary, preferred_element_type=jnp.float32)
        + jnp.einsum("shr,spr->shp", turned_mine, rotary, preferred_element_type=jnp.float32)
    ) * score_scale
    scores = lax.psum(partial_value.astype(jnp.bfloat16), "tp").astype(jnp.float32)
    attention = jax.nn.softmax(scores, axis=-1).astype(jnp.bfloat16)
    context = jnp.einsum(
        "shp,spc->shc", attention, hidden_summary, preferred_element_type=jnp.float32
    ).astype(jnp.bfloat16)

    def project_heads(row_start, row_count):
        part_context = lax.dynamic_slice_in_dim(context, row_start, row_count, 1)
        part_weight = lax.dynamic_slice_in_dim(payload_widening, row_start, row_count, 1)
        return jnp.einsum(
            "shc,chv->hsv", part_context, part_weight, preferred_element_type=jnp.float32
        )

    values = summed_rows(project_heads, head_each, "tp")
    first_read = rescaled_lines(values.transpose(1, 0, 2)).astype(jnp.bfloat16)
    return (hidden_summary, rotary, first_read)


def solution(mesh):
    return jax.shard_map(
        shards,
        mesh=mesh,
        in_specs=(
            P(None, ("sp", "tp"), None),
            P(),
            P(),
            P(),
            P(),
            P("tp", None, None),
            P("tp", None, None),
            P("sp", "tp", None),
            P("sp", "tp", None),
        ),
        out_specs=(P("sp", None, "tp"), P("sp", None, "tp"), P("sp", "tp", None)),
        check_vma=False,
    )
```

profile of v0, /device:TPU:0, one launch (start us, length us, event | category | flops | bytes accessed | tf_op | source)
XLA Modules:
  0.0 55.6 jit_solution(11520406021461989264)
XLA Ops:
  0.7 1.7 %fusion = f32[8,32]{1,0:T(8,128)S(1)} fusion(bf16[8,32,2048]{2,1,0:T(8,128)(2,1)} %param.9), kind=kLoop, calls=%fused_computation.2 | loop fusion | flops 1572608 | bytes 1049600 | tf_op jit(solution)/shard_map/reduce_sum | solution.py:18
  2.4 1.5 %fusion.2 = bf16[8,32,2048]{2,1,0:T(8,128)(2,1)S(1)} fusion(bf16[8,32,2048]{2,1,0:T(8,128)(2,1)} %param.9, f32[2048]{0:T(1024)} %param.10, f32[8,32]{1,0:T(8,128)S(1)} %add_rsqrt_fusion), kind=kLoop, calls=%fused_computation.4 | loop fusion | flops 2097152 | bytes 2106368 | tf_op jit(solution)/shard_map/convert_element_type | solution.py:62
  4.0 0.4 fusion.6
  4.5 0.1 multiply_cosine_fusion
  4.6 0.1 subtract_convert_fusion
  4.9 0.1 copy.34
  5.0 0.8 %reshape.300 = bf16[32,2,256]{2,1,0:T(2,128)(2,1)} reshape(bf16[32,1,16,32]{3,2,1,0:T(8,128)(2,1)S(1)} %bitcast.62) | data formatting | bytes 65536
  5.8 7.3 %all-to-all-start.1 = ((bf16[32,2,256]{2,1,0:T(2,128)(2,1)}), bf16[32,2,256]{2,1,0:T(2,128)(2,1)S(1)}, u32[]{:S(2)}, u32[]{:S(2)}) async-start(bf16[32,2,256]{2,1,0:T(2,128)(2,1)} %reshape.300), calls=%async_computation.1 | async-start | bytes 65536 | tf_op jit(solution)/shard_map/all_to_all | solution.py:89
  13.1 5.2 %all_gather.7 = bf16[1,16,64]{2,0,1:T(2,128)(2,1)S(1)} all-gather(bf16[1,4,64]{2,0,1:T(2,128)(2,1)S(1)} %copy.37), channel_id=1, replica_groups=mesh['sp'=8,'tp'=4] {'tp'}, dimensions={1}, use_global_device_ids=true | all-gather | bytes 2560 | tf_op jit(solution)/shard_map/all_gather | solution.py:104
  18.3 0.8 %multiply_reduce_fusion = (f32[256]{0:T(256)S(1)}, f32[256,512]{1,0:T(8,128)S(1)}) fusion(bf16[256,2048]{1,0:T(8,128)(2,1)S(1)} %bitcast.57, bf16[2048,512]{1,0:T(8,128)(2,1)S(1)} %copy-done), kind=kOutput, calls=%fused_computation.20 | convolution fusion | flops 537394944 | bytes 3671040 | tf_op jit(solution)/shard_map/dot_general | solution.py:64
  19.2 0.1 multiply_convert_fusion
  19.4 0.8 %copy.31 = bf16[8,1,32,4,128]{4,2,3,0,1:T(8,128)(2,1)} copy(bf16[8,1,32,4,128]{4,3,2,0,1:T(4,128)(2,1)S(1)} %reshape_reshape.3) | data formatting | bytes 524288 | tf_op jit(solution)/shard_map/reshape;reshape | solution.py:42
  20.1 0.2 all-to-all-done.1
  20.4 5.6 %all-to-all-start = ((bf16[32,1,32,128]{3,2,1,0:T(8,128)(2,1)}), bf16[32,1,32,128]{3,2,1,0:T(8,128)(2,1)S(1)}, u32[]{:S(2)}, u32[]{:S(2)}) async-start(bf16[32,1,32,128]{3,2,1,0:T(8,128)(2,1)} %bitcast.3), calls=%async_computation | async-start | bytes 524288 | tf_op jit(solution)/shard_map/all_to_all | solution.py:82
  26.1 0.6 %dynamic-slice = u32[1]{0:T(128)} dynamic-slice(u32[32]{0:T(128)S(1)} %copy-done.7, u32[]{:T(128)S(6)} %add.73), dynamic_slice_sizes={1} | dynamic-slice | bytes 12
  27.3 5.2 %all_gather.6 = bf16[1,16,128]{2,0,1:T(2,128)(2,1)S(1)} all-gather(bf16[1,4,128]{2,0,1:T(2,128)(2,1)S(1)} %copy.36), channel_id=1, replica_groups=mesh['sp'=8,'tp'=4] {'tp'}, dimensions={1}, use_global_device_ids=true | all-gather | bytes 5120 | tf_op jit(solution)/shard_map/all_gather | solution.py:103
  32.6 0.4 fusion.11
  33.0 0.2 reshape.301
  33.2 0.2 reshape.287
  33.3 0.8 %squeeze.7 = bf16[1,1024,16]{1,2,0:T(8,128)(2,1)} reshape(bf16[32,1,32,16]{2,0,3,1:T(8,128)(2,1)S(1)} %copy.35) | data formatting | bytes 65536 | tf_op jit(solution)/shard_map/squeeze | solution.py:98
  34.1 2.4 %all-to-all-done = bf16[32,1,32,128]{3,2,1,0:T(8,128)(2,1)S(1)} async-done(((bf16[32,1,32,128]{3,2,1,0:T(8,128)(2,1)}), bf16[32,1,32,128]{3,2,1,0:T(8,128)(2,1)S(1)}, u32[]{:S(2)}, u32[]{:S(2)}) %all-to-all-start) | async-done | bytes 262176 | tf_op jit(solution)/shard_map/all_to_all | solution.py:82
  36.5 0.2 fusion.25
  36.7 0.2 fusion.7
  36.9 10.6 %psum.7 = bf16[1,16,1024]{2,1,0:T(8,128)(2,1)S(1)} all-reduce(bf16[1,16,1024]{2,1,0:T(8,128)(2,1)S(1)} %fusion.7), channel_id=1, replica_groups=mesh['sp'=8,'tp'=4] {'tp'}, use_global_device_ids=true, to_apply=%region_2.0 | all-reduce | flops 16384 | bytes 65536 | tf_op jit(solution)/shard_map/psum | solution.py:118
  47.5 0.1 reduce_max.14
  47.7 0.2 fusion.13
  47.9 0.2 fusion.8
  48.1 0.3 fusion.9
  48.3 5.8 %all-reduce = f32[16,1,128]{2,0,1:T(8,128)S(1)} all-reduce(f32[16,1,128]{2,0,1:T(8,128)S(1)} %bitcast.64), channel_id=2, replica_groups=mesh['sp'=8,'tp'=4] {'tp'}, use_global_device_ids=true, to_apply=%region_5.0.clone | all-reduce | flops 2048 | bytes 16384
  54.1 0.1 multiply_reduce_fusion.1
  54.2 0.6 %multiply_convert_fusion.1 = bf16[1,4,128]{2,1,0:T(4,128)(2,1)} fusion(f32[16,1,128]{2,0,1:T(8,128)S(1)} %all-reduce, u32[]{:T(128)S(6)} %multiply.33, f32[4]{0:T(128)S(1)} %add_rsqrt_fusion.2), kind=kLoop, calls=%fused_computation.46 | loop fusion | flops 1024 | bytes 3092 | tf_op jit(solution)/shard_map/convert_element_type | solution.py:132
  54.9 0.7 %copy.56 = bf16[1,1024,128]{2,1,0:T(8,128)(2,1)} copy(bf16[1,1024,128]{2,1,0:T(8,128)(2,1)S(1)} %bitcast.60) | data formatting | bytes 524288
  (31 shorter events, 0.5 us)
Async XLA Ops:
  0.6 17.7 %copy-start = (bf16[2048,512]{1,0:T(8,128)(2,1)S(1)}, bf16[2048,512]{1,0:T(8,128)(2,1)}, u32[]{:S(2)}) copy-start(bf16[2048,512]{1,0:T(8,128)(2,1)} %param.11) | copy-start | bytes 6291460
  0.6 3.3 %copy-start.1 = (bf16[2048,64]{0,1:T(8,128)(2,1)S(1)}, bf16[2048,64]{0,1:T(8,128)(2,1)}, u32[]{:S(2)}) copy-start(bf16[2048,64]{0,1:T(8,128)(2,1)} %param.12) | copy-start | bytes 786436
  2.4 10.7 %copy-start.3 = (bf16[1,4,64]{2,1,0:T(4,128)(2,1)S(1)}, bf16[1,4,64]{2,1,0:T(4,128)(2,1)}, u32[]{:S(2)}) copy-start(bf16[1,4,64]{2,1,0:T(4,128)(2,1)} %param.17) | copy-start | bytes 1540
  5.0 14.2 %copy-start.2 = (f32[512]{0:T(512)S(1)}, f32[512]{0:T(512)}, u32[]{:S(2)}) copy-start(f32[512]{0:T(512)} %param.13) | copy-start | bytes 6148
  5.8 14.6 %all-to-all-start.1 = ((bf16[32,2,256]{2,1,0:T(2,128)(2,1)}), bf16[32,2,256]{2,1,0:T(2,128)(2,1)S(1)}, u32[]{:S(2)}, u32[]{:S(2)}) async-start(bf16[32,2,256]{2,1,0:T(2,128)(2,1)} %reshape.300), calls=%async_computation.1 | async-start | bytes 65536 | tf_op jit(solution)/shard_map/all_to_all | solution.py:89
  19.1 6.9 %copy-start.4 = (bf16[1,4,128]{2,1,0:T(4,128)(2,1)S(1)}, bf16[1,4,128]{2,1,0:T(4,128)(2,1)}, u32[]{:S(2)}) copy-start(bf16[1,4,128]{2,1,0:T(4,128)(2,1)} %param.16) | copy-start | bytes 3076
  19.1 7.0 %copy-start.7 = (u32[32]{0:T(128)S(1)}, u32[32]{0:T(128)}, u32[]{:S(2)}) copy-start(u32[32]{0:T(128)} %constant.54) | copy-start | bytes 388
  19.1 13.5 %copy-start.5 = (bf16[128,16,128]{2,1,0:T(8,128)(2,1)S(1)}, bf16[128,16,128]{2,1,0:T(8,128)(2,1)}, u32[]{:S(2)}) copy-start(bf16[128,16,128]{2,1,0:T(8,128)(2,1)} %param.14) | copy-start | bytes 1572868
  19.4 28.7 %copy-start.6 = (bf16[128,16,128]{2,1,0:T(8,128)(2,1)S(1)}, bf16[128,16,128]{2,1,0:T(8,128)(2,1)}, u32[]{:S(2)}) copy-start(bf16[128,16,128]{2,1,0:T(8,128)(2,1)} %param.15) | copy-start | bytes 1572868
  20.4 16.2 %all-to-all-start = ((bf16[32,1,32,128]{3,2,1,0:T(8,128)(2,1)}), bf16[32,1,32,128]{3,2,1,0:T(8,128)(2,1)S(1)}, u32[]{:S(2)}, u32[]{:S(2)}) async-start(bf16[32,1,32,128]{3,2,1,0:T(8,128)(2,1)} %bitcast.3), calls=%async_computation | async-start | bytes 524288 | tf_op jit(solution)/shard_map/all_to_all | solution.py:82
where the time goes:
time: 55.9 us; the launch traced here: 55.6 us
  blocking collectives  26.7 us (48%)
  starting transfers between devices  12.9 us (23%)
  other arithmetic  4.95 us (9%)
  local copies, waits for them, and re-layouts  4.3 us (8%)
  waiting for transfers between devices  2.64 us (5%)
  matrix products  2.46 us (4%)
  between operations  1.56 us (3%)
    psum x1, blocking collectives, shards(): lax.psum(partial_value.astype(jnp.bfloat16), 'tp').astype(jnp.float32)  10.6 us
    all_to_all x1, starting transfers between devices, shards(): lax.all_to_all(to_pieces(rotary, sp_count, tp_count), ('sp', 'tp'), split...  7.33 us
    unnamed x1, blocking collectives  5.76 us
    all_to_all x1, starting transfers between devices, shards(): lax.all_to_all(to_pieces(hidden_summary, sp_count, tp_count), ('sp', 'tp'...  5.61 us
    all_gather x1, blocking collectives, shards(): lax.all_gather(query_nope, 'tp', axis=1, tiled=True)  5.2 us
    all_gather x1, blocking collectives, shards(): lax.all_gather(query_rotary, 'tp', axis=1, tiled=True)  5.19 us
    all_to_all x1, waiting for transfers between devices, shards(): lax.all_to_all(to_pieces(hidden_summary, sp_count, tp_count), ('sp', 'tp'...  2.41 us
    unnamed x22, local copies, waits for them, and re-layouts  2.26 us
  transfers between devices with their start and end apart: 2, of which 2 were waited for; matrix products, arithmetic and copies ran while one was open for 7% of the time, Pallas kernels for 0%

commit v1 on v0

--- a/solution.py
+++ b/solution.py
@@ -55,6 +55,10 @@
     query_nope,
     query_rotary,
 ):
+
+    def enter_tables(w_in, axis_key="tp"):
+        return jnp.sum(lax.all_gather(w_in, axis_name=axis_key), axis=0)
+
     seq_count, pos_local, feature_width = layer_input.shape
     sp_count = lax.axis_size("sp")
     tp_count = lax.axis_size("tp")
@@ -115,7 +119,7 @@
         jnp.einsum("shc,spc->shp", absorbed, hidden_summary, preferred_element_type=jnp.float32)
         + jnp.einsum("shr,spr->shp", turned_mine, rotary, preferred_element_type=jnp.float32)
     ) * score_scale
-    scores = lax.psum(partial_value.astype(jnp.bfloat16), "tp").astype(jnp.float32)
+    scores = enter_tables(partial_value.astype(jnp.bfloat16)).astype(jnp.float32)
     attention = jax.nn.softmax(scores, axis=-1).astype(jnp.bfloat16)
     context = jnp.einsum(
         "shp,spc->shc", attention, hidden_summary, preferred_element_type=jnp.float32

time: 55.9 us -> 51.1 us (0.914)
  blocking collectives: 26.7 us -> 21.9 us
    psum x1 -> x0, blocking collectives: 10.6 us -> none  [shards(): lax.psum(partial_value.astype(jnp.bfloat16), 'tp').astype(jnp.float32)]
    all_gather x0 -> x1, blocking collectives: none -> 5.41 us  [enter_tables(): return jnp.sum(lax.all_gather(w_in, axis_name=axis_key), axis=0)]
  transfers between devices with their start and end apart: 2 -> 2, of which waited for: 2 -> 2; matrix products, arithmetic and copies ran while one was open for 7% -> 8% of each run, Pallas kernels for 0% -> 0%
where the time goes in v1:
time: 51.1 us; the launch traced here: 50.8 us
  blocking collectives  21.9 us (43%)
  starting transfers between devices  12.9 us (25%)
  other arithmetic  4.97 us (10%)
  local copies, waits for them, and re-layouts  4.3 us (8%)
  waiting for transfers between devices  2.64 us (5%)
  matrix products  2.46 us (5%)
  between operations  1.56 us (3%)
    all_to_all x1, starting transfers between devices, shards(): lax.all_to_all(to_pieces(rotary, sp_count, tp_count), ('sp', 'tp'), split...  7.33 us
    unnamed x1, blocking collectives  6.08 us
    all_to_all x1, starting transfers between devices, shards(): lax.all_to_all(to_pieces(hidden_summary, sp_count, tp_count), ('sp', 'tp'...  5.61 us
    all_gather x1, blocking collectives, enter_tables(): return jnp.sum(lax.all_gather(w_in, axis_name=axis_key), axis=0)  5.41 us
    all_gather x1, blocking collectives, shards(): lax.all_gather(query_nope, 'tp', axis=1, tiled=True)  5.2 us
    all_gather x1, blocking collectives, shards(): lax.all_gather(query_rotary, 'tp', axis=1, tiled=True)  5.19 us
    all_to_all x1, waiting for transfers between devices, shards(): lax.all_to_all(to_pieces(hidden_summary, sp_count, tp_count), ('sp', 'tp'...  2.41 us
    unnamed x22, local copies, waits for them, and re-layouts  2.26 us
  transfers between devices with their start and end apart: 2, of which 2 were waited for; matrix products, arithmetic and copies ran while one was open for 8% of the time, Pallas kernels for 0%

profile of v1, /device:TPU:0, one launch (start us, length us, event | category | flops | bytes accessed | tf_op | source)
XLA Modules:
  0.0 50.8 jit_solution(15715659774731488801)
XLA Ops:
  0.7 1.7 %fusion = f32[8,32]{1,0:T(8,128)S(1)} fusion(bf16[8,32,2048]{2,1,0:T(8,128)(2,1)} %param.9), kind=kLoop, calls=%fused_computation.2 | loop fusion | flops 1572608 | bytes 1049600 | tf_op jit(solution)/shard_map/reduce_sum | solution.py:18
  2.4 1.5 %fusion.2 = bf16[8,32,2048]{2,1,0:T(8,128)(2,1)S(1)} fusion(bf16[8,32,2048]{2,1,0:T(8,128)(2,1)} %param.9, f32[2048]{0:T(1024)} %param.10, f32[8,32]{1,0:T(8,128)S(1)} %add_rsqrt_fusion), kind=kLoop, calls=%fused_computation.4 | loop fusion | flops 2097152 | bytes 2106368 | tf_op jit(solution)/shard_map/convert_element_type | solution.py:66
  4.0 0.4 fusion.6
  4.5 0.1 multiply_cosine_fusion
  4.6 0.1 subtract_convert_fusion
  4.9 0.1 copy.43
  5.0 0.8 %reshape.407 = bf16[32,2,256]{2,1,0:T(2,128)(2,1)} reshape(bf16[32,1,16,32]{3,2,1,0:T(8,128)(2,1)S(1)} %bitcast.83) | data formatting | bytes 65536
  5.8 7.3 %all-to-all-start.1 = ((bf16[32,2,256]{2,1,0:T(2,128)(2,1)}), bf16[32,2,256]{2,1,0:T(2,128)(2,1)S(1)}, u32[]{:S(2)}, u32[]{:S(2)}) async-start(bf16[32,2,256]{2,1,0:T(2,128)(2,1)} %reshape.407), calls=%async_computation.1 | async-start | bytes 65536 | tf_op jit(solution)/shard_map/all_to_all | solution.py:93
  13.1 5.2 %all_gather.13 = bf16[1,16,64]{2,0,1:T(2,128)(2,1)S(1)} all-gather(bf16[1,4,64]{2,0,1:T(2,128)(2,1)S(1)} %copy.46), channel_id=1, replica_groups=mesh['sp'=8,'tp'=4] {'tp'}, dimensions={1}, use_global_device_ids=true | all-gather | bytes 2560 | tf_op jit(solution)/shard_map/all_gather | solution.py:108
  18.3 0.8 %multiply_reduce_fusion = (f32[256]{0:T(256)S(1)}, f32[256,512]{1,0:T(8,128)S(1)}) fusion(bf16[256,2048]{1,0:T(8,128)(2,1)S(1)} %bitcast.77, bf16[2048,512]{1,0:T(8,128)(2,1)S(1)} %copy-done), kind=kOutput, calls=%fused_computation.19 | convolution fusion | flops 537394944 | bytes 3671040 | tf_op jit(solution)/shard_map/dot_general | solution.py:68
  19.2 0.1 multiply_convert_fusion
  19.4 0.8 %copy.40 = bf16[8,1,32,4,128]{4,2,3,0,1:T(8,128)(2,1)} copy(bf16[8,1,32,4,128]{4,3,2,0,1:T(4,128)(2,1)S(1)} %reshape_reshape.3) | data formatting | bytes 524288 | tf_op jit(solution)/shard_map/reshape;reshape | solution.py:42
  20.1 0.2 all-to-all-done.1
  20.4 5.6 %all-to-all-start = ((bf16[32,1,32,128]{3,2,1,0:T(8,128)(2,1)}), bf16[32,1,32,128]{3,2,1,0:T(8,128)(2,1)S(1)}, u32[]{:S(2)}, u32[]{:S(2)}) async-start(bf16[32,1,32,128]{3,2,1,0:T(8,128)(2,1)} %bitcast.3), calls=%async_computation | async-start | bytes 524288 | tf_op jit(solution)/shard_map/all_to_all | solution.py:86
  26.1 0.6 %dynamic-slice = u32[1]{0:T(128)} dynamic-slice(u32[32]{0:T(128)S(1)} %copy-done.7, u32[]{:T(128)S(6)} %add.71), dynamic_slice_sizes={1} | dynamic-slice | bytes 12
  27.3 5.2 %all_gather.12 = bf16[1,16,128]{2,0,1:T(2,128)(2,1)S(1)} all-gather(bf16[1,4,128]{2,0,1:T(2,128)(2,1)S(1)} %copy.45), channel_id=1, replica_groups=mesh['sp'=8,'tp'=4] {'tp'}, dimensions={1}, use_global_device_ids=true | all-gather | bytes 5120 | tf_op jit(solution)/shard_map/all_gather | solution.py:107
  32.6 0.4 fusion.10
  33.0 0.2 reshape.408
  33.2 0.2 reshape.391
  33.3 0.8 %squeeze.7 = bf16[1,1024,16]{1,2,0:T(8,128)(2,1)} reshape(bf16[32,1,32,16]{2,0,3,1:T(8,128)(2,1)S(1)} %copy.44) | data formatting | bytes 65536 | tf_op jit(solution)/shard_map/squeeze | solution.py:102
  34.1 2.4 %all-to-all-done = bf16[32,1,32,128]{3,2,1,0:T(8,128)(2,1)S(1)} async-done(((bf16[32,1,32,128]{3,2,1,0:T(8,128)(2,1)}), bf16[32,1,32,128]{3,2,1,0:T(8,128)(2,1)S(1)}, u32[]{:S(2)}, u32[]{:S(2)}) %all-to-all-start) | async-done | bytes 262176 | tf_op jit(solution)/shard_map/all_to_all | solution.py:86
  36.5 0.2 fusion.30
  36.7 0.2 fusion.5
  36.9 5.4 %all-gather = bf16[64,1024]{1,0:T(8,128)(2,1)S(1)} all-gather(bf16[16,1024]{1,0:T(8,128)(2,1)S(1)} %fusion.5), channel_id=2, replica_groups=mesh['sp'=8,'tp'=4] {'tp'}, dimensions={0}, use_global_device_ids=true | all-gather | bytes 163840 | tf_op jit(solution)/shard_map/all_gather | solution.py:60
  42.4 0.1 reduce_max.14
  42.5 0.2 fusion.18
  42.7 0.2 fusion.7
  42.9 0.3 fusion.8
  43.2 6.1 %all-reduce = f32[16,1,128]{2,0,1:T(8,128)S(1)} all-reduce(f32[16,1,128]{2,0,1:T(8,128)S(1)} %bitcast.85), channel_id=3, replica_groups=mesh['sp'=8,'tp'=4] {'tp'}, use_global_device_ids=true, to_apply=%region_5.0.clone | all-reduce | flops 2048 | bytes 16384
  49.3 0.1 multiply_reduce_fusion.1
  49.4 0.6 %multiply_convert_fusion.1 = bf16[1,4,128]{2,1,0:T(4,128)(2,1)} fusion(f32[16,1,128]{2,0,1:T(8,128)S(1)} %all-reduce, u32[]{:T(128)S(6)} %multiply.33, f32[4]{0:T(128)S(1)} %add_rsqrt_fusion.2), kind=kLoop, calls=%fused_computation.51 | loop fusion | flops 1024 | bytes 3092 | tf_op jit(solution)/shard_map/convert_element_type | solution.py:136
  50.0 0.7 %copy.65 = bf16[1,1024,128]{2,1,0:T(8,128)(2,1)} copy(bf16[1,1024,128]{2,1,0:T(8,128)(2,1)S(1)} %bitcast.80) | data formatting | bytes 524288
  (32 shorter events, 0.5 us)
Async XLA Ops:
  0.6 17.7 %copy-start = (bf16[2048,512]{1,0:T(8,128)(2,1)S(1)}, bf16[2048,512]{1,0:T(8,128)(2,1)}, u32[]{:S(2)}) copy-start(bf16[2048,512]{1,0:T(8,128)(2,1)} %param.11) | copy-start | bytes 6291460
  0.6 3.3 %copy-start.1 = (bf16[2048,64]{0,1:T(8,128)(2,1)S(1)}, bf16[2048,64]{0,1:T(8,128)(2,1)}, u32[]{:S(2)}) copy-start(bf16[2048,64]{0,1:T(8,128)(2,1)} %param.12) | copy-start | bytes 786436
  2.4 10.7 %copy-start.3 = (bf16[1,4,64]{2,1,0:T(4,128)(2,1)S(1)}, bf16[1,4,64]{2,1,0:T(4,128)(2,1)}, u32[]{:S(2)}) copy-start(bf16[1,4,64]{2,1,0:T(4,128)(2,1)} %param.17) | copy-start | bytes 1540
  5.0 14.2 %copy-start.2 = (f32[512]{0:T(512)S(1)}, f32[512]{0:T(512)}, u32[]{:S(2)}) copy-start(f32[512]{0:T(512)} %param.13) | copy-start | bytes 6148
  5.8 14.6 %all-to-all-start.1 = ((bf16[32,2,256]{2,1,0:T(2,128)(2,1)}), bf16[32,2,256]{2,1,0:T(2,128)(2,1)S(1)}, u32[]{:S(2)}, u32[]{:S(2)}) async-start(bf16[32,2,256]{2,1,0:T(2,128)(2,1)} %reshape.407), calls=%async_computation.1 | async-start | bytes 65536 | tf_op jit(solution)/shard_map/all_to_all | solution.py:93
  19.1 6.9 %copy-start.4 = (bf16[1,4,128]{2,1,0:T(4,128)(2,1)S(1)}, bf16[1,4,128]{2,1,0:T(4,128)(2,1)}, u32[]{:S(2)}) copy-start(bf16[1,4,128]{2,1,0:T(4,128)(2,1)} %param.16) | copy-start | bytes 3076
  19.1 7.0 %copy-start.7 = (u32[32]{0:T(128)S(1)}, u32[32]{0:T(128)}, u32[]{:S(2)}) copy-start(u32[32]{0:T(128)} %constant.56) | copy-start | bytes 388
  19.1 13.5 %copy-start.5 = (bf16[128,16,128]{2,1,0:T(8,128)(2,1)S(1)}, bf16[128,16,128]{2,1,0:T(8,128)(2,1)}, u32[]{:S(2)}) copy-start(bf16[128,16,128]{2,1,0:T(8,128)(2,1)} %param.14) | copy-start | bytes 1572868
  19.4 23.6 %copy-start.6 = (bf16[128,16,128]{2,1,0:T(8,128)(2,1)S(1)}, bf16[128,16,128]{2,1,0:T(8,128)(2,1)}, u32[]{:S(2)}) copy-start(bf16[128,16,128]{2,1,0:T(8,128)(2,1)} %param.15) | copy-start | bytes 1572868
  20.4 16.2 %all-to-all-start = ((bf16[32,1,32,128]{3,2,1,0:T(8,128)(2,1)}), bf16[32,1,32,128]{3,2,1,0:T(8,128)(2,1)S(1)}, u32[]{:S(2)}, u32[]{:S(2)}) async-start(bf16[32,1,32,128]{3,2,1,0:T(8,128)(2,1)} %bitcast.3), calls=%async_computation | async-start | bytes 524288 | tf_op jit(solution)/shard_map/all_to_all | solution.py:86
